TPU v7x, 512 devices: a 4x2x32 block of a 4x8x32 slice. The times are simulated.
512 devices in a mesh: grp: 2 (over y), fs: 32 (over z), tp: 8 (over x, core).
Axes of the slice: x: 4, y: 2, z: 32, core: 2. Of those that a mesh axis runs over, the one named last changes fastest.
The devices are a block of a 4x8x32 slice.
Arguments:
- tokens: bfloat16 [32768, 2048], P(('grp', 'fs'), 'tp'), parts along dimension 0, may hold values from -6 to 6
- first_gain: bfloat16 [2048], replicated, may hold values from 0.099609375 to 1.8984375
- u_proj: bfloat16 [2048, 1024], P('fs', 'tp'), may hold values from -0.125 to 0.125
- v_proj: bfloat16 [2048, 1024], P('fs', 'tp'), may hold values from -0.125 to 0.125
- group_gain: bfloat16 [8, 128], P('tp'), may hold values from 0.099609375 to 1.8984375
- spatial: bfloat16 [8, 128, 128], P('tp'), may hold values from -0.5 to 0.5
- spatial_bias: bfloat16 [8, 128], P('tp'), may hold values from 0.099609375 to 1.8984375
- mix_proj: bfloat16 [1024, 2048], P('fs', 'tp'), may hold values from -0.1875 to 0.1875
- second_gain: bfloat16 [2048], replicated, may hold values from 0.099609375 to 1.8984375
- up_proj: bfloat16 [2048, 8192], P('fs', 'tp'), may hold values from -0.125 to 0.125
- down_proj: bfloat16 [8192, 2048], P('tp', 'fs'), may hold values from -0.0625 to 0.0625
Outputs:
- layer_out: bfloat16 [32768, 2048], P(('grp', 'fs'), 'tp'), parts along dimension 0
There are 2 independent parts, one for each index of `grp`. A program takes and returns all parts, laid end to end along the dimension named above; an argument that names none is the same for every part. Nothing has to cross between parts.
All inputs are finite; a program needn't handle non-finite values.
Results may differ from a plain program's by a relative error of at most 0.017.
Values may be sent and summed in bfloat16 or wider, within the bound.
No kernel may reach another device: no remote copies, remote signals or barrier semaphores. Data moves between devices by JAX's collectives and lax.ppermute only.
A program may use at most 64 MiB of HBM per device.

v0:
```python
import jax
import jax.numpy as jnp
from jax import lax
from jax.sharding import PartitionSpec as P

EPS = 1e-06


def sent_to_all(shard, axis):
    copies = jnp.broadcast_to(shard, (lax.axis_size(axis), *shard.shape))
    return lax.all_to_all(copies, axis, split_axis=0, concat_axis=0, tiled=True)


def in_order(blocks, dim):
    blocks = jnp.moveaxis(blocks, 0, dim)
    lengths = blocks.shape
    return blocks.reshape(*lengths[:dim], lengths[dim] * lengths[dim + 1], *lengths[dim + 2 :])


def collect(shard, axis, dim):
    blocks = sent_to_all(shard, axis)
    return in_order(blocks, dim)


def side_by_side(arrays, axis, dim, along):
    both = jnp.concatenate(arrays, axis=along)
    result, at, outs = (lax.all_gather(both, axis, axis=dim, tiled=True), 0, [])
    for a in arrays:
        outs.append(lax.slice_in_dim(result, at, at + a.shape[along], axis=along))
        at += a.shape[along]
    return tuple(outs)


def split_up(shard, dim, size):
    lengths = shard.shape
    blocks = shard.reshape(*lengths[:dim], size, lengths[dim] // size, *lengths[dim + 1 :])
    return jnp.moveaxis(blocks, dim, 0)


def sum_at_owner(shard, axis, dim):
    size = lax.axis_size(axis)
    blocks = lax.all_to_all(split_up(shard, dim, size), axis, 0, 0, tiled=True)
    return jnp.sum(blocks.astype(jnp.float32), axis=0)


def rms_scale(values, gain_vec):
    mean_sq = jnp.mean(values * values, axis=-1, keepdims=True)
    return values * lax.rsqrt(mean_sq + EPS) * gain_vec.astype(jnp.float32)


def per_device(
    tokens,
    first_gain,
    u_proj,
    v_proj,
    group_gain,
    spatial,
    spatial_bias,
    mix_proj,
    second_gain,
    up_proj,
    down_proj,
):
    up_collected = lax.all_gather(up_proj, "fs", axis=0, tiled=True)
    whole_rows = collect(tokens, "tp", 1)
    row_count = whole_rows.shape[0]
    normed_rows = rms_scale(whole_rows.astype(jnp.float32), first_gain).astype(jnp.bfloat16)
    local_width = u_proj.shape[1]
    weight_parts = side_by_side((u_proj, v_proj), "fs", 0, 1)
    column_part = normed_rows
    u_pre = jnp.dot(column_part, weight_parts[0], preferred_element_type=jnp.float32)
    v_pre = jnp.dot(column_part, weight_parts[1], preferred_element_type=jnp.float32)
    u_act = jax.nn.gelu(u_pre).astype(jnp.bfloat16)
    local_groups = group_gain.shape[0]
    group_width = group_gain.shape[1]
    v_groups = jax.nn.gelu(v_pre).reshape(row_count, local_groups, group_width)
    v_normed = rms_scale(v_groups, group_gain).astype(jnp.bfloat16)
    block_len = spatial.shape[1]
    block_view = v_normed.reshape(row_count // block_len, block_len, local_groups, group_width)
    causal_mask = jnp.tril(jnp.ones((block_len, block_len), jnp.bool_))
    masked_weights = jnp.where(causal_mask[None], spatial, jnp.zeros_like(spatial))
    mixed_vals = jnp.einsum(
        "gts,nsgd->ntgd", masked_weights, block_view, preferred_element_type=jnp.float32
    )
    mixed_vals = mixed_vals + spatial_bias.astype(jnp.float32).T[None, :, :, None]
    gated_vals = (u_act.astype(jnp.float32) * mixed_vals.reshape(row_count, local_width)).astype(
        jnp.bfloat16
    )
    gated_whole = collect(gated_vals, "tp", 1)
    column_part = gated_whole
    mix_vals = jnp.dot(
        column_part,
        lax.all_gather(mix_proj, "fs", axis=0, tiled=True),
        preferred_element_type=jnp.float32,
    )
    mid_stream = (tokens.astype(jnp.float32) + mix_vals).astype(jnp.bfloat16)
    mid_whole = collect(mid_stream, "tp", 1)
    normed_two = rms_scale(mid_whole.astype(jnp.float32), second_gain).astype(jnp.bfloat16)
    pre_act = jnp.dot(normed_two, up_collected, preferred_element_type=jnp.float32)
    hidden_act = jnp.square(jax.nn.relu(pre_act)).astype(jnp.bfloat16)
    down_terms = jnp.dot(
        hidden_act,
        lax.all_gather(down_proj, "fs", axis=1, tiled=True),
        preferred_element_type=jnp.float32,
    )
    down_sum = sum_at_owner(down_terms.astype(jnp.bfloat16), "tp", 1)
    return (mid_stream.astype(jnp.float32) + down_sum).astype(jnp.bfloat16)


def solution(mesh):
    return jax.shard_map(
        per_device,
        mesh=mesh,
        in_specs=(
            P(("grp", "fs"), "tp"),
            P(),
            P("fs", "tp"),
            P("fs", "tp"),
            P("tp", None),
            P("tp", None, None),
            P("tp", None),
            P("fs", "tp"),
            P(),
            P("fs", "tp"),
            P("tp", "fs"),
        ),
        out_specs=P(("grp", "fs"), "tp"),
        check_vma=False,
    )
```

profile of v0, /device:TPU:33, one launch (start us, length us, event | category | flops | bytes accessed | tf_op | source)
XLA Modules:
  0.0 485.8 jit_solution(16322225659080245963)
XLA Ops:
  6.6 1.4 pad_maximum_fusion
  8.0 0.7 all-gather.6.cloned.1.call-update
  8.8 1.1 copy.15
  9.9 1.5 broadcast_in_dim.10
  11.4 45.1 %all-to-all-start = ((bf16[8,512,256]{1,2,0:T(8,128)(2,1)}), bf16[8,512,256]{1,2,0:T(8,128)(2,1)S(1)}, u32[]{:S(2)}, u32[]{:S(2)}) async-start(bf16[8,512,256]{1,2,0:T(8,128)(2,1)} %broadcast_in_dim.10), calls=%async_computation | async-start | bytes 4194304 | tf_op jit(solution)/shard_map/all_to_all | solution.py:11
  56.5 0.7 all-gather.8.cloned.1.call-update
  57.3 25.5 %all-to-all-done = bf16[8,512,256]{1,2,0:T(8,128)(2,1)S(1)} async-done(((bf16[8,512,256]{1,2,0:T(8,128)(2,1)}), bf16[8,512,256]{1,2,0:T(8,128)(2,1)S(1)}, u32[]{:S(2)}, u32[]{:S(2)}) %all-to-all-start) | async-done | bytes 2097184 | tf_op jit(solution)/shard_map/all_to_all | solution.py:11
  82.8 0.5 multiply_reduce_fusion.1
  83.3 1.9 fusion.3
  85.2 63.5 %all-gather.4.cloned.1.call-done = bf16[2048,256]{1,0:T(8,128)(2,1)} async-done(((bf16[64,256]{1,0:T(8,128)(2,1)}), bf16[2048,256]{1,0:T(8,128)(2,1)}) %all-gather.4.cloned.1.call-update) | async-done | bytes 1048592 | tf_op jit(solution)/shard_map/all_gather | solution.py:27
  148.8 2.6 multiply_reduce_fusion.2
  151.4 0.1 multiply_convert_fusion.1
  151.5 0.2 fusion.5
  151.7 0.8 fusion.28
  152.5 0.1 copy.16
  152.6 1.2 broadcast_in_dim.12
  153.8 25.8 %all-to-all-start.1 = ((bf16[8,512,128]{1,2,0:T(8,128)(2,1)}), bf16[8,512,128]{1,2,0:T(8,128)(2,1)S(1)}, u32[]{:S(2)}, u32[]{:S(2)}) async-start(bf16[8,512,128]{1,2,0:T(8,128)(2,1)} %broadcast_in_dim.12), calls=%async_computation.1 | async-start | bytes 2097152 | tf_op jit(solution)/shard_map/all_to_all | solution.py:11
  179.6 45.6 %all_gather.13 = bf16[1024,256]{1,0:T(8,128)(2,1)S(1)} all-gather(bf16[32,256]{1,0:T(8,128)(2,1)S(1)} %copy-done.3), channel_id=1, replica_groups=mesh['grp'=2,'fs'=32,'tp'=8] {'fs'}, dimensions={0}, use_global_device_ids=true | all-gather | bytes 540672 | tf_op jit(solution)/shard_map/all_gather | solution.py:93
  225.2 0.5 fusion.4
  225.7 0.1 copy.17
  225.8 1.5 broadcast_in_dim.13
  227.4 17.1 %all-to-all-start.2 = ((bf16[8,512,256]{1,2,0:T(8,128)(2,1)}), bf16[8,512,256]{1,2,0:T(8,128)(2,1)S(1)}, u32[]{:S(2)}, u32[]{:S(2)}) async-start(bf16[8,512,256]{1,2,0:T(8,128)(2,1)} %broadcast_in_dim.13), calls=%async_computation.2 | async-start | bytes 4194304 | tf_op jit(solution)/shard_map/all_to_all | solution.py:11
  244.5 26.2 %all-to-all-done.2 = bf16[8,512,256]{1,2,0:T(8,128)(2,1)S(1)} async-done(((bf16[8,512,256]{1,2,0:T(8,128)(2,1)}), bf16[8,512,256]{1,2,0:T(8,128)(2,1)S(1)}, u32[]{:S(2)}, u32[]{:S(2)}) %all-to-all-start.2) | async-done | bytes 2097184 | tf_op jit(solution)/shard_map/all_to_all | solution.py:11
  270.7 0.5 multiply_reduce_fusion
  271.2 1.9 fusion.1
  273.1 12.1 %all-gather.6.cloned.1.call-done = bf16[2048,1024]{1,0:T(8,128)(2,1)} async-done(((bf16[64,1024]{1,0:T(8,128)(2,1)}), bf16[2048,1024]{1,0:T(8,128)(2,1)}) %all-gather.6.cloned.1.call-update) | async-done | bytes 4194320 | tf_op jit(solution)/shard_map/all_gather | solution.py:64
  285.2 133.1 %all-gather.8.cloned.1.call-done = bf16[1024,2048]{0,1:T(8,128)(2,1)} async-done(((bf16[1024,64]{0,1:T(8,128)(2,1)}), bf16[1024,2048]{0,1:T(8,128)(2,1)}) %all-gather.8.cloned.1.call-update) | async-done | bytes 4194320 | tf_op jit(solution)/shard_map/all_gather | solution.py:103
  418.3 8.6 %convolution_convert_fusion = bf16[512,2048]{1,0:T(8,128)(2,1)S(1)} fusion(bf16[1024,2048]{0,1:T(8,128)(2,1)} %all-gather.8.cloned.1.call-done, bf16[512,2048]{0,1:T(8,128)(2,1)} %fusion.1, bf16[2048,1024]{1,0:T(8,128)(2,1)} %all-gather.6.cloned.1.call-done), kind=kOutput, calls=%fused_computation.9 | convolution fusion | flops 4297588736 | bytes 12582912 | tf_op jit(solution)/shard_map/dot_general | solution.py:101
  426.9 0.1 copy.21
  427.0 51.2 %all_to_all.20 = bf16[8,512,256]{2,1,0:T(8,128)(2,1)S(1)} all-to-all(bf16[8,512,256]{2,1,0:T(8,128)(2,1)S(1)} %bitcast.52), channel_id=1, replica_groups=mesh['grp'=2,'fs'=32,'tp'=8] {'tp'}, dimensions={0} | all-to-all | bytes 4194304 | tf_op jit(solution)/shard_map/all_to_all | solution.py:42
  478.2 0.3 convert_reduce_fusion
  478.5 0.8 add_convert_fusion
  (30 shorter events, 0.2 us)
Async XLA Ops:
  6.5 142.2 %all-gather.4.cloned.1.call-start = ((), (), s32[]{:S(2)}) async-start(), calls=%async_computation.4 | async-start | bytes 1081344 | tf_op jit(solution)/shard_map/all_gather | solution.py:27
  8.0 277.3 %all-gather.6.cloned.1.call-start = ((), (), s32[]{:S(2)}) async-start(), calls=%async_computation.5 | async-start | bytes 4325376 | tf_op jit(solution)/shard_map/all_gather | solution.py:64
  11.4 45.8 %copy-start.4 = (bf16[2048]{0:T(1024)(128)(2,1)S(1)}, bf16[2048]{0:T(1024)(128)(2,1)}, u32[]{:S(2)}) copy-start(bf16[2048]{0:T(1024)(128)(2,1)} %param.12) | copy-start | bytes 12292
  11.4 45.9 %copy-start.7 = (bf16[1,128]{1,0:T(2,128)(2,1)S(1)}, bf16[1,128]{1,0:T(2,128)(2,1)}, u32[]{:S(2)}) copy-start(bf16[1,128]{1,0:T(2,128)(2,1)} %param.15) | copy-start | bytes 772
  11.4 45.9 %copy-start.8 = (bf16[1,128]{1,0:T(2,128)(2,1)S(1)}, bf16[1,128]{1,0:T(2,128)(2,1)}, u32[]{:S(2)}) copy-start(bf16[1,128]{1,0:T(2,128)(2,1)} %param.17) | copy-start | bytes 772
  11.4 71.4 %all-to-all-start = ((bf16[8,512,256]{1,2,0:T(8,128)(2,1)}), bf16[8,512,256]{1,2,0:T(8,128)(2,1)S(1)}, u32[]{:S(2)}, u32[]{:S(2)}) async-start(bf16[8,512,256]{1,2,0:T(8,128)(2,1)} %broadcast_in_dim.10), calls=%async_computation | async-start | bytes 4194304 | tf_op jit(solution)/shard_map/all_to_all | solution.py:11
  56.5 361.8 %all-gather.8.cloned.1.call-start = ((), (), s32[]{:S(2)}) async-start(), calls=%async_computation.6 | async-start | bytes 4325376 | tf_op jit(solution)/shard_map/all_gather | solution.py:103
  85.2 66.3 %copy-start.2 = (bf16[1,128,128]{2,1,0:T(8,128)(2,1)S(1)}, bf16[1,128,128]{2,1,0:T(8,128)(2,1)}, u32[]{:S(2)}) copy-start(bf16[1,128,128]{2,1,0:T(8,128)(2,1)} %param.16) | copy-start | bytes 98308
  85.2 66.5 %copy-start = (bf16[512,2048]{0,1:T(8,128)(2,1)S(1)}, bf16[512,2048]{0,1:T(8,128)(2,1)}, u32[]{:S(2)}) copy-start(bf16[512,2048]{0,1:T(8,128)(2,1)} %fusion.3) | copy-start | bytes 6291460
  148.8 3.0 copy-start.6
  152.5 27.1 %copy-start.3 = (bf16[32,256]{1,0:T(8,128)(2,1)S(1)}, bf16[32,256]{1,0:T(8,128)(2,1)}, u32[]{:S(2)}) copy-start(bf16[32,256]{1,0:T(8,128)(2,1)} %param.18) | copy-start | bytes 49156
  152.5 72.7 %copy-start.1 = (bf16[512,256]{1,0:T(8,128)(2,1)S(1)}, bf16[512,256]{1,0:T(8,128)(2,1)}, u32[]{:S(2)}) copy-start(bf16[512,256]{1,0:T(8,128)(2,1)} %param.11) | copy-start | bytes 786436
  153.8 71.4 %all-to-all-start.1 = ((bf16[8,512,128]{1,2,0:T(8,128)(2,1)}), bf16[8,512,128]{1,2,0:T(8,128)(2,1)S(1)}, u32[]{:S(2)}, u32[]{:S(2)}) async-start(bf16[8,512,128]{1,2,0:T(8,128)(2,1)} %broadcast_in_dim.12), calls=%async_computation.1 | async-start | bytes 2097152 | tf_op jit(solution)/shard_map/all_to_all | solution.py:11
  227.4 17.1 %copy-start.5 = (bf16[2048]{0:T(1024)(128)(2,1)S(1)}, bf16[2048]{0:T(1024)(128)(2,1)}, u32[]{:S(2)}) copy-start(bf16[2048]{0:T(1024)(128)(2,1)} %param.19) | copy-start | bytes 12292
  227.4 43.3 %all-to-all-start.2 = ((bf16[8,512,256]{1,2,0:T(8,128)(2,1)}), bf16[8,512,256]{1,2,0:T(8,128)(2,1)S(1)}, u32[]{:S(2)}, u32[]{:S(2)}) async-start(bf16[8,512,256]{1,2,0:T(8,128)(2,1)} %broadcast_in_dim.13), calls=%async_computation.2 | async-start | bytes 4194304 | tf_op jit(solution)/shard_map/all_to_all | solution.py:11
Sparse Core Ops, SparseCore 0:
  9.4 139.2 all-gather.3
  150.8 134.3 all-gather.5
  287.3 130.9 all-gather.7
where the time goes:
time: 486 us
  waiting for transfers between devices  262 us (54%)
  blocking collectives  96.8 us (20%)
  starting transfers between devices  88 us (18%)
  between operations  13.3 us (3%)
  matrix products  12.6 us (3%)
  other arithmetic  7.45 us (2%)
  local copies, waits for them, and re-layouts  5.77 us (1%)
    all_gather x1, waiting for transfers between devices, per_device(): lax.all_gather(down_proj, 'fs', axis=1, tiled=True)  133 us
    all_to_all x3, starting transfers between devices, sent_to_all(): return lax.all_to_all(copies, axis, split_axis=0, concat_axis=0, tiled=True)  88 us
    all_gather x1, waiting for transfers between devices, side_by_side(): result, at, outs = (lax.all_gather(both, axis, axis=dim, tiled=True), 0, [])  63.5 us
    all_to_all x3, waiting for transfers between devices, sent_to_all(): return lax.all_to_all(copies, axis, split_axis=0, concat_axis=0, tiled=True)  51.7 us
    all_to_all x1, blocking collectives, sum_at_owner(): blocks = lax.all_to_all(split_up(shard, dim, size), axis, 0, 0, tiled=True)  51.2 us
    all_gather x1, blocking collectives, per_device(): lax.all_gather(mix_proj, 'fs', axis=0, tiled=True)  45.6 us
    all_gather x1, waiting for transfers between devices, per_device(): up_collected = lax.all_gather(up_proj, 'fs', axis=0, tiled=True)  12.1 us
  transfers between devices with their start and end apart: 6, of which 5 were waited for; matrix products, arithmetic and copies ran while one was open for 3% of the time, Pallas kernels for 0%

commit v1 on v0

v1 whole, which is shorter than its diff:
```python
import jax
import jax.numpy as jnp
from jax import lax
from jax.sharding import PartitionSpec as P

EPS = 1e-06


def rms_scale(values, gain_vec):
    mean_sq = jnp.mean(values * values, axis=-1, keepdims=True)
    return values * lax.rsqrt(mean_sq + EPS) * gain_vec.astype(jnp.float32)


def sent_to_all(shard, axis):
    copies = jnp.broadcast_to(shard, (lax.axis_size(axis), *shard.shape))
    return lax.all_to_all(copies, axis, split_axis=0, concat_axis=0, tiled=True)


def in_order(blocks, dim):
    blocks = jnp.moveaxis(blocks, 0, dim)
    lengths = blocks.shape
    return blocks.reshape(*lengths[:dim], lengths[dim] * lengths[dim + 1], *lengths[dim + 2 :])


def split_up(shard, dim, size):
    lengths = shard.shape
    blocks = shard.reshape(*lengths[:dim], size, lengths[dim] // size, *lengths[dim + 1 :])
    return jnp.moveaxis(blocks, dim, 0)


def sum_at_owner(shard, axis, dim):
    size = lax.axis_size(axis)
    blocks = lax.all_to_all(split_up(shard, dim, size), axis, 0, 0, tiled=True)
    return jnp.sum(blocks.astype(jnp.float32), axis=0)


def shift(x, axis, by):
    n = lax.axis_size(axis)
    return lax.ppermute(x, axis, [(i, (i + by) % n) for i in range(n)])


def gather_two_level(shard, axis):
    n = lax.axis_size(axis)
    half = n // 2
    own = lax.all_gather(
        shard, axis, axis=0, tiled=False,
        axis_index_groups=[[r + 2 * i for i in range(half)] for r in range(2)],
    )
    cut = half // 2
    from_left = shift(own[:cut], axis, 1)
    from_right = shift(own[cut:], axis, -1)
    other = jnp.concatenate([from_left, from_right], 0)
    odd = lax.axis_index(axis) % 2 == 1
    even_set = jnp.where(odd, other, own)
    odd_set = jnp.where(odd, own, other)
    return jnp.stack([even_set, odd_set], 1).reshape(n, *shard.shape)


def swap_cores(x, axis):
    n = lax.axis_size(axis)
    return lax.ppermute(x, axis, [(i, i ^ 1) for i in range(n)])


def gather_chips(x, axis):
    n = lax.axis_size(axis)
    return lax.all_gather(
        x, axis, axis=0, tiled=False,
        axis_index_groups=[[2 * i + c for i in range(n // 2)] for c in range(2)],
    )


def pair_up(mine, theirs, axis):
    second = lax.axis_index(axis) % 2 == 1
    first_core = jnp.where(second, theirs, mine)
    second_core = jnp.where(second, mine, theirs)
    both = jnp.stack([first_core, second_core], 1)
    return both.reshape(-1, *mine.shape[1:])


def per_device(
    tokens,
    first_gain,
    u_proj,
    v_proj,
    group_gain,
    spatial,
    spatial_bias,
    mix_proj,
    second_gain,
    up_proj,
    down_proj,
):
    ffn_w = lax.all_gather(jnp.stack([up_proj, down_proj.T]), "fs", axis=1, tiled=True)
    whole_rows = in_order(sent_to_all(tokens, "tp"), 1)
    small = jnp.concatenate([jnp.concatenate([u_proj, v_proj], 1), mix_proj], 0)
    small_all = gather_two_level(small, "fs")
    rows_uv = u_proj.shape[0]
    width = u_proj.shape[1]
    uv = small_all[:, :rows_uv].reshape(-1, 2 * width)
    mix = small_all[:, rows_uv:].reshape(-1, mix_proj.shape[1])

    row_count = whole_rows.shape[0]
    normed_rows = rms_scale(whole_rows.astype(jnp.float32), first_gain).astype(jnp.bfloat16)
    uv_pre = jnp.dot(normed_rows, uv, preferred_element_type=jnp.float32)
    u_act = jax.nn.gelu(uv_pre[:, :width]).astype(jnp.bfloat16)
    local_groups, group_width = group_gain.shape
    v_groups = jax.nn.gelu(uv_pre[:, width:]).reshape(row_count, local_groups, group_width)
    v_normed = rms_scale(v_groups, group_gain).astype(jnp.bfloat16)
    block_len = spatial.shape[1]
    block_view = v_normed.reshape(row_count // block_len, block_len, local_groups, group_width)
    causal_mask = jnp.tril(jnp.ones((block_len, block_len), jnp.bool_))
    masked_weights = jnp.where(causal_mask[None], spatial, jnp.zeros_like(spatial))
    mixed_vals = jnp.einsum(
        "gts,nsgd->ntgd", masked_weights, block_view, preferred_element_type=jnp.float32
    )
    mixed_vals = mixed_vals + spatial_bias.astype(jnp.float32).T[None, :, :, None]
    gated_vals = (u_act.astype(jnp.float32) * mixed_vals.reshape(row_count, width)).astype(
        jnp.bfloat16
    )
    g_mine = gather_chips(gated_vals, "tp")
    gated_whole = in_order(pair_up(g_mine, swap_cores(g_mine, "tp"), "tp"), 1)
    mix_vals = jnp.dot(gated_whole, mix, preferred_element_type=jnp.float32)
    mid_stream = (tokens.astype(jnp.float32) + mix_vals).astype(jnp.bfloat16)
    cut = row_count // 2
    m_mine = jnp.concatenate(
        [gather_chips(mid_stream[:cut], "tp"), gather_chips(mid_stream[cut:], "tp")], 1
    )
    mid_whole = in_order(pair_up(m_mine, swap_cores(m_mine, "tp"), "tp"), 1)
    normed_two = rms_scale(mid_whole.astype(jnp.float32), second_gain).astype(jnp.bfloat16)
    pre_act = jnp.dot(normed_two, ffn_w[0], preferred_element_type=jnp.float32)
    hidden_act = jnp.square(jax.nn.relu(pre_act)).astype(jnp.bfloat16)
    down_terms = lax.dot_general(
        hidden_act, ffn_w[1], (((1,), (1,)), ((), ())), preferred_element_type=jnp.float32
    )
    down_sum = sum_at_owner(down_terms.astype(jnp.bfloat16), "tp", 1)
    return (mid_stream.astype(jnp.float32) + down_sum).astype(jnp.bfloat16)


def solution(mesh):
    return jax.shard_map(
        per_device,
        mesh=mesh,
        in_specs=(
            P(("grp", "fs"), "tp"),
            P(),
            P("fs", "tp"),
            P("fs", "tp"),
            P("tp", None),
            P("tp", None, None),
            P("tp", None),
            P("fs", "tp"),
            P(),
            P("fs", "tp"),
            P("tp", "fs"),
        ),
        out_specs=P(("grp", "fs"), "tp"),
        check_vma=False,
    )
```

time: 486 us -> 245 us (0.50)
  waiting for transfers between devices: 262 us -> 16.9 us
  blocking collectives: 96.8 us -> 116 us
  starting transfers between devices: 88 us -> 70.4 us
    all_gather x3 -> x1, waiting for transfers between devices: 209 us -> 0.01 us  [per_device(): lax.all_gather(jnp.stack([up_proj, down_proj.T]), 'fs', axis=1, tiled=True)]
    all_to_all x3 -> x1, waiting for transfers between devices: 51.7 us -> 0.01 us  [sent_to_all(): return lax.all_to_all(copies, axis, split_axis=0, concat_axis=0, tiled=True)]
    all_to_all x3 -> x1, starting transfers between devices: 88 us -> 45.1 us  [sent_to_all(): return lax.all_to_all(copies, axis, split_axis=0, concat_axis=0, tiled=True)]
    all_gather x1 -> x4, blocking collectives: 45.6 us -> 75.2 us  [the longest x1 41.5 us: gather_two_level(): lax.all_gather(shard, axis, axis=0, tiled=False, axis_index_groups=[[r +...]
    ppermute x0 -> x4, starting transfers between devices: none -> 25.4 us  [the longest x2 16.3 us: swap_cores(): return lax.ppermute(x, axis, [(i, i ^ 1) for i in range(n)])]
    ppermute x0 -> x4, waiting for transfers between devices: none -> 16.8 us  [the longest x2 14.4 us: shift(): return lax.ppermute(x, axis, [(i, (i + by) % n) for i in range(n)])]
    all_to_all x1, blocking collectives: 51.2 us -> 41.1 us  [sum_at_owner(): blocks = lax.all_to_all(split_up(shard, dim, size), axis, 0, 0, tiled=True)]
    dot_general x4 -> x3, matrix products: 12.4 us -> 9.81 us  [the longest x1 8.58 us: per_device(): lax.dot_general(hidden_act, ffn_w[1], (((1,), (1,)), ((), ())), preferred...]
  transfers between devices with their start and end apart: 6 -> 6, of which waited for: 5 -> 4; matrix products, arithmetic and copies ran while one was open for 3% -> 6% of each run, Pallas kernels for 0% -> 0%
where the time goes in v1:
time: 245 us; the launch traced here: 244 us
  blocking collectives  116 us (47%)
  starting transfers between devices  70.4 us (29%)
  waiting for transfers between devices  16.9 us (7%)
  between operations  13.8 us (6%)
  local copies, waits for them, and re-layouts  10.5 us (4%)
  matrix products  9.98 us (4%)
  other arithmetic  6.56 us (3%)
    all_to_all x1, starting transfers between devices, sent_to_all(): return lax.all_to_all(copies, axis, split_axis=0, concat_axis=0, tiled=True)  45.1 us
    all_gather x1, blocking collectives, gather_two_level(): lax.all_gather(shard, axis, axis=0, tiled=False, axis_index_groups=[[r +...  41.5 us
    all_to_all x1, blocking collectives, sum_at_owner(): blocks = lax.all_to_all(split_up(shard, dim, size), axis, 0, 0, tiled=True)  41.1 us
    all_gather x3, blocking collectives, gather_chips(): lax.all_gather(x, axis, axis=0, tiled=False, axis_index_groups=[[2 * i +...  33.7 us
    ppermute x2, starting transfers between devices, swap_cores(): return lax.ppermute(x, axis, [(i, i ^ 1) for i in range(n)])  16.3 us
    ppermute x2, waiting for transfers between devices, shift(): return lax.ppermute(x, axis, [(i, (i + by) % n) for i in range(n)])  14.4 us
    ppermute x2, starting transfers between devices, shift(): return lax.ppermute(x, axis, [(i, (i + by) % n) for i in range(n)])  9.1 us
    dot_general x1, matrix products, per_device(): lax.dot_general(hidden_act, ffn_w[1], (((1,), (1,)), ((), ())), preferred...  8.58 us
  transfers between devices with their start and end apart: 6, of which 4 were waited for; matrix products, arithmetic and copies ran while one was open for 6% of the time, Pallas kernels for 0%

profile of v1, /device:TPU:33, one launch (start us, length us, event | category | flops | bytes accessed | tf_op | source)
XLA Modules:
  0.0 244.4 jit_solution(16497261841629519899)
XLA Ops:
  6.6 1.7 pad_maximum_fusion.4
  8.3 1.1 copy.18
  9.4 1.5 broadcast_in_dim.5
  11.0 45.1 %all-to-all-start = ((bf16[8,512,256]{1,2,0:T(8,128)(2,1)}), bf16[8,512,256]{1,2,0:T(8,128)(2,1)S(1)}, u32[]{:S(2)}, u32[]{:S(2)}) async-start(bf16[8,512,256]{1,2,0:T(8,128)(2,1)} %broadcast_in_dim.5), calls=%async_computation | async-start | bytes 4194304 | tf_op jit(solution)/shard_map/all_to_all | solution.py:16
  56.1 41.5 %all-gather = bf16[1536,256]{1,0:T(8,128)(2,1)S(1)} all-gather(bf16[96,256]{1,0:T(8,128)(2,1)S(1)} %pad_maximum_fusion.5), channel_id=2, replica_groups={{0,16,32,48,64,80,96,112,128,144,160,176,192,208,224,240},{8,24,40,56,7..., dimensions={0}, use_global_device_ids=true | all-gather | bytes 835584 | tf_op jit(solution)/shard_map/all_gather | solution.py:45
  97.6 0.9 fusion.35
  98.6 7.1 %collective-permute-start = (bf16[8,96,256]{2,1,0:T(8,128)(2,1)}, bf16[8,96,256]{2,1,0:T(8,128)(2,1)}, u32[]{:S(2)}, u32[]{:S(2)}) collective-permute-start(bf16[8,96,256]{2,1,0:T(8,128)(2,1)} %bitcast.2), channel_id=1, source_target_pairs={{0,8},{8,16},{16,24},{24,32},{32,40},{40,48},{48,56},{56,64},{64,7... | collective-permute-start | bytes 1179656 | tf_op jit(solution)/shard_map/ppermute | solution.py:39
  105.7 2.0 collective-permute-start.1
  107.8 13.6 %collective-permute-done = bf16[8,96,256]{2,1,0:T(8,128)(2,1)} collective-permute-done((bf16[8,96,256]{2,1,0:T(8,128)(2,1)}, bf16[8,96,256]{2,1,0:T(8,128)(2,1)}, u32[]{:S(2)}, u32[]{:S(2)}) %collective-permute-start) | collective-permute-done | bytes 393248 | tf_op jit(solution)/shard_map/ppermute | solution.py:39
  121.3 1.0 constant_dynamic-update-slice_fusion.1
  122.4 0.8 collective-permute-done.1
  123.6 1.1 copy-done
  124.8 0.5 fusion
  125.3 0.5 fusion.2
  125.9 0.7 fusion.37
  127.3 10.7 %all-gather.1 = bf16[2048,128]{1,0:T(8,128)(2,1)S(1)} all-gather(bf16[512,128]{1,0:T(8,128)(2,1)S(1)} %fusion.28), channel_id=3, replica_groups={{0,2,4,6},{1,3,5,7},{8,10,12,14},{9,11,13,15},{16,18,20,22},{17,19,21,2..., dimensions={0}, use_global_device_ids=true | all-gather | bytes 655360 | tf_op jit(solution)/shard_map/all_gather | solution.py:66
  138.0 10.6 %collective-permute-start.2 = (bf16[4,512,128]{2,1,0:T(8,128)(2,1)S(1)}, bf16[4,512,128]{2,1,0:T(8,128)(2,1)S(1)}, u32[]{:S(2)}, u32[]{:S(2)}) collective-permute-start(bf16[4,512,128]{2,1,0:T(8,128)(2,1)S(1)} %bitcast.102), channel_id=1, source_target_pairs={{0,1},{1,0},{2,3},{3,2},{4,5},{5,4},{6,7},{7,6},{8,9},{9,8},{10,11... | collective-permute-start | bytes 1572872 | tf_op jit(solution)/shard_map/ppermute | solution.py:61
  148.7 1.1 slice.47
  149.7 0.4 collective-permute-done.2
  150.3 0.5 copy.21
  151.2 0.5 fusion.10
  151.7 11.2 %all-gather.2 = bf16[1024,256]{1,0:T(8,128)(2,1)S(1)} all-gather(bf16[256,256]{1,0:T(8,128)(2,1)S(1)} %get-tuple-element.13), channel_id=4, replica_groups={{0,2,4,6},{1,3,5,7},{8,10,12,14},{9,11,13,15},{16,18,20,22},{17,19,21,2..., dimensions={0}, use_global_device_ids=true | all-gather | bytes 655360 | tf_op jit(solution)/shard_map/all_gather | solution.py:66
  162.9 11.8 %all-gather.3 = bf16[1024,256]{1,0:T(8,128)(2,1)S(1)} all-gather(bf16[256,256]{1,0:T(8,128)(2,1)S(1)} %get-tuple-element.14), channel_id=5, replica_groups={{0,2,4,6},{1,3,5,7},{8,10,12,14},{9,11,13,15},{16,18,20,22},{17,19,21,2..., dimensions={0}, use_global_device_ids=true | all-gather | bytes 655360 | tf_op jit(solution)/shard_map/all_gather | solution.py:66
  174.8 5.6 %collective-permute-start.3 = (bf16[4,512,256]{2,1,0:T(8,128)(2,1)S(1)}, bf16[4,512,256]{2,1,0:T(8,128)(2,1)S(1)}, u32[]{:S(2)}, u32[]{:S(2)}) collective-permute-start(bf16[4,512,256]{2,1,0:T(8,128)(2,1)S(1)} %pad_maximum_fusion.3), channel_id=1, source_target_pairs={{0,1},{1,0},{2,3},{3,2},{4,5},{5,4},{6,7},{7,6},{8,9},{9,8},{10,11... | collective-permute-start | bytes 3145736 | tf_op jit(solution)/shard_map/ppermute | solution.py:61
  180.4 2.1 collective-permute-done.3
  182.5 0.4 select_bitcast_fusion.1
  183.1 0.5 fusion.3
  183.6 0.6 fusion.9
  184.2 2.5 %copy.23 = bf16[512,8,256]{0,2,1:T(8,128)(2,1)} copy(bf16[512,8,256]{2,0,1:T(8,128)(2,1)S(1)} %fusion.9) | data formatting | bytes 4194304 | tf_op jit(solution)/shard_map/convert_element_type | solution.py:129
  186.7 8.6 %fusion.8 = bf16[512,2048]{1,0:T(8,128)(2,1)S(1)} fusion(bf16[2,2048,1024]{2,1,0:T(8,128)(2,1)} %all-gather.6.cloned.1.call-done, bf16[512,2048]{0,1:T(8,128)(2,1)} %bitcast.104), kind=kOutput, calls=%fused_computation.15 | convolution fusion | flops 4297588736 | bytes 12582912 | tf_op jit(solution)/shard_map/dot_general | solution.py:132
  195.4 41.1 %all_to_all.10 = bf16[8,512,256]{2,1,0:T(8,128)(2,1)S(1)} all-to-all(bf16[8,512,256]{2,1,0:T(8,128)(2,1)S(1)} %bitcast.92), channel_id=1, replica_groups=mesh['grp'=2,'fs'=32,'tp'=8] {'tp'}, dimensions={0} | all-to-all | bytes 4194304 | tf_op jit(solution)/shard_map/all_to_all | solution.py:33
  236.8 0.8 add_convert_fusion
  (46 shorter events, 2.4 us)
Async XLA Ops:
  6.5 180.2 %all-gather.6.cloned.1.call-start = ((), (), s32[]{:S(2)}) async-start(), calls=%async_computation.2 | async-start | bytes 8650752 | tf_op jit(solution)/shard_map/all_gather | solution.py:93
  11.0 45.1 %copy-start.3 = (bf16[32,256]{1,0:T(8,128)(2,1)S(1)}, bf16[32,256]{1,0:T(8,128)(2,1)}, u32[]{:S(2)}) copy-start(bf16[32,256]{1,0:T(8,128)(2,1)} %param.18) | copy-start | bytes 49156
  11.0 45.1 %copy-start.4 = (bf16[64,128]{1,0:T(8,128)(2,1)S(1)}, bf16[64,128]{1,0:T(8,128)(2,1)}, u32[]{:S(2)}) copy-start(bf16[64,128]{1,0:T(8,128)(2,1)} %param.14) | copy-start | bytes 49156
  11.0 45.1 %copy-start.5 = (bf16[64,128]{1,0:T(8,128)(2,1)S(1)}, bf16[64,128]{1,0:T(8,128)(2,1)}, u32[]{:S(2)}) copy-start(bf16[64,128]{1,0:T(8,128)(2,1)} %param.13) | copy-start | bytes 49156
  11.0 113.8 %all-to-all-start = ((bf16[8,512,256]{1,2,0:T(8,128)(2,1)}), bf16[8,512,256]{1,2,0:T(8,128)(2,1)S(1)}, u32[]{:S(2)}, u32[]{:S(2)}) async-start(bf16[8,512,256]{1,2,0:T(8,128)(2,1)} %broadcast_in_dim.5), calls=%async_computation | async-start | bytes 4194304 | tf_op jit(solution)/shard_map/all_to_all | solution.py:16
  56.1 51.6 %copy-start.8 = (bf16[1,128]{1,0:T(2,128)(2,1)S(1)}, bf16[1,128]{1,0:T(2,128)(2,1)}, u32[]{:S(2)}) copy-start(bf16[1,128]{1,0:T(2,128)(2,1)} %param.15) | copy-start | bytes 772
  56.1 51.6 %copy-start.6 = (bf16[2048]{0:T(1024)(128)(2,1)S(1)}, bf16[2048]{0:T(1024)(128)(2,1)}, u32[]{:S(2)}) copy-start(bf16[2048]{0:T(1024)(128)(2,1)} %param.12) | copy-start | bytes 12292
  56.1 51.7 %copy-start.9 = (bf16[1,128]{1,0:T(2,128)(2,1)S(1)}, bf16[1,128]{1,0:T(2,128)(2,1)}, u32[]{:S(2)}) copy-start(bf16[1,128]{1,0:T(2,128)(2,1)} %param.17) | copy-start | bytes 772
  98.6 22.8 %collective-permute-start = (bf16[8,96,256]{2,1,0:T(8,128)(2,1)}, bf16[8,96,256]{2,1,0:T(8,128)(2,1)}, u32[]{:S(2)}, u32[]{:S(2)}) collective-permute-start(bf16[8,96,256]{2,1,0:T(8,128)(2,1)} %bitcast.2), channel_id=1, source_target_pairs={{0,8},{8,16},{16,24},{24,32},{32,40},{40,48},{48,56},{56,64},{64,7... | collective-permute-start | bytes 1179656 | tf_op jit(solution)/shard_map/ppermute | solution.py:39
  105.7 17.4 %collective-permute-start.1 = (bf16[8,96,256]{2,1,0:T(8,128)(2,1)}, bf16[8,96,256]{2,1,0:T(8,128)(2,1)S(1)}, u32[]{:S(2)}, u32[]{:S(2)}) collective-permute-start(bf16[8,96,256]{2,1,0:T(8,128)(2,1)} %bitcast.3), channel_id=1, source_target_pairs={{0,248},{8,0},{16,8},{24,16},{32,24},{40,32},{48,40},{56,48},{64,5... | collective-permute-start | bytes 1179656 | tf_op jit(solution)/shard_map/ppermute | solution.py:39
  123.5 1.2 copy-start
  125.9 1.1 copy-start.2
  138.0 12.1 %collective-permute-start.2 = (bf16[4,512,128]{2,1,0:T(8,128)(2,1)S(1)}, bf16[4,512,128]{2,1,0:T(8,128)(2,1)S(1)}, u32[]{:S(2)}, u32[]{:S(2)}) collective-permute-start(bf16[4,512,128]{2,1,0:T(8,128)(2,1)S(1)} %bitcast.102), channel_id=1, source_target_pairs={{0,1},{1,0},{2,3},{3,2},{4,5},{5,4},{6,7},{7,6},{8,9},{9,8},{10,11... | collective-permute-start | bytes 1572872 | tf_op jit(solution)/shard_map/ppermute | solution.py:61
  150.2 1.0 copy-start.1
  151.7 28.7 %copy-start.7 = (bf16[2048]{0:T(1024)(128)(2,1)S(1)}, bf16[2048]{0:T(1024)(128)(2,1)}, u32[]{:S(2)}) copy-start(bf16[2048]{0:T(1024)(128)(2,1)} %param.19) | copy-start | bytes 12292
  174.8 7.7 %collective-permute-start.3 = (bf16[4,512,256]{2,1,0:T(8,128)(2,1)S(1)}, bf16[4,512,256]{2,1,0:T(8,128)(2,1)S(1)}, u32[]{:S(2)}, u32[]{:S(2)}) collective-permute-start(bf16[4,512,256]{2,1,0:T(8,128)(2,1)S(1)} %pad_maximum_fusion.3), channel_id=1, source_target_pairs={{0,1},{1,0},{2,3},{3,2},{4,5},{5,4},{6,7},{7,6},{8,9},{9,8},{10,11... | collective-permute-start | bytes 3145736 | tf_op jit(solution)/shard_map/ppermute | solution.py:61
Sparse Core Ops, SparseCore 0:
  9.4 173.3 all-gather.5

commit v2 on v1

--- a/solution.py
+++ b/solution.py
@@ -1,6 +1,8 @@
 import jax
 import jax.numpy as jnp
 from jax import lax
+from jax.experimental import pallas as pl
+from jax.experimental.pallas import tpu as pltpu
 from jax.sharding import PartitionSpec as P
 
 EPS = 1e-06
@@ -20,18 +22,6 @@
     blocks = jnp.moveaxis(blocks, 0, dim)
     lengths = blocks.shape
     return blocks.reshape(*lengths[:dim], lengths[dim] * lengths[dim + 1], *lengths[dim + 2 :])
-
-
-def split_up(shard, dim, size):
-    lengths = shard.shape
-    blocks = shard.reshape(*lengths[:dim], size, lengths[dim] // size, *lengths[dim + 1 :])
-    return jnp.moveaxis(blocks, dim, 0)
-
-
-def sum_at_owner(shard, axis, dim):
-    size = lax.axis_size(axis)
-    blocks = lax.all_to_all(split_up(shard, dim, size), axis, 0, 0, tiled=True)
-    return jnp.sum(blocks.astype(jnp.float32), axis=0)
 
 
 def shift(x, axis, by):
@@ -61,20 +51,162 @@
     return lax.ppermute(x, axis, [(i, i ^ 1) for i in range(n)])
 
 
-def gather_chips(x, axis):
-    n = lax.axis_size(axis)
-    return lax.all_gather(
-        x, axis, axis=0, tiled=False,
-        axis_index_groups=[[2 * i + c for i in range(n // 2)] for c in range(2)],
-    )
-
-
-def pair_up(mine, theirs, axis):
-    second = lax.axis_index(axis) % 2 == 1
-    first_core = jnp.where(second, theirs, mine)
-    second_core = jnp.where(second, mine, theirs)
-    both = jnp.stack([first_core, second_core], 1)
-    return both.reshape(-1, *mine.shape[1:])
+def chip_groups(axis):
+    n = lax.axis_size(axis)
+    return [[2 * i + c for i in range(n // 2)] for c in range(2)]
+
+
+def exchange_chips(blocks, axis):
+    return lax.all_to_all(
+        blocks, axis, split_axis=0, concat_axis=0, tiled=True,
+        axis_index_groups=chip_groups(axis),
+    )
+
+
+NT = (((1,), (1,)), ((), ()))
+
+
+def mix_kernel(core_ref, mine_ref, theirs_ref, mix_ref, tok_ref, out_ref):
+    core = core_ref[0]
+    chips = mine_ref.shape[0]
+    total = tok_ref[...].astype(jnp.float32)
+    for x in range(chips):
+        total += jnp.dot(mine_ref[x], mix_ref[2 * x + core], preferred_element_type=jnp.float32)
+        total += jnp.dot(
+            theirs_ref[x], mix_ref[2 * x + 1 - core], preferred_element_type=jnp.float32
+        )
+    mid = total.astype(out_ref.dtype)
+    for x in range(chips):
+        out_ref[x] = mid
+
+
+def mix_to_mid(core, mine, theirs, mix, tokens):
+    chips, rows, width = mine.shape
+    cols = tokens.shape[1]
+    step = rows // 4
+    return pl.pallas_call(
+        mix_kernel,
+        grid_spec=pltpu.PrefetchScalarGridSpec(
+            num_scalar_prefetch=1,
+            grid=(4,),
+            in_specs=[
+                pl.BlockSpec((chips, step, width), lambda i, c: (0, i, 0)),
+                pl.BlockSpec((chips, step, width), lambda i, c: (0, i, 0)),
+                pl.BlockSpec((2 * chips, width, cols), lambda i, c: (0, 0, 0)),
+                pl.BlockSpec((step, cols), lambda i, c: (i, 0)),
+            ],
+            out_specs=pl.BlockSpec((chips, step, cols), lambda i, c: (0, i, 0)),
+        ),
+        out_shape=jax.ShapeDtypeStruct((chips, rows, cols), tokens.dtype),
+        cost_estimate=pl.CostEstimate(
+            flops=4 * chips * rows * width * cols, bytes_accessed=4 << 20, transcendentals=0
+        ),
+    )(core, mine, theirs, mix.reshape(2 * chips, width, cols), tokens)
+
+
+def norm_kernel(core_ref, mine_ref, theirs_ref, gain_ref, out_ref):
+    core = core_ref[0]
+    chips, _, cols = mine_ref.shape
+    square = 0.0
+    for x in range(chips):
+        a = mine_ref[x].astype(jnp.float32)
+        b = theirs_ref[x].astype(jnp.float32)
+        square += jnp.sum(a * a + b * b, axis=1, keepdims=True)
+    scale = lax.rsqrt(square / (2 * chips * cols) + EPS)
+    for x in range(chips):
+        for ref, c in ((mine_ref, core), (theirs_ref, 1 - core)):
+            at = pl.ds(pl.multiple_of((2 * x + c) * cols, cols), cols)
+            gain = gain_ref[:, at].astype(jnp.float32)
+            out_ref[:, at] = (ref[x].astype(jnp.float32) * scale * gain).astype(out_ref.dtype)
+
+
+def norm_pieces(core, mine, theirs, gain):
+    chips, rows, cols = mine.shape
+    step = rows // 4
+    whole = 2 * chips * cols
+    return pl.pallas_call(
+        norm_kernel,
+        grid_spec=pltpu.PrefetchScalarGridSpec(
+            num_scalar_prefetch=1,
+            grid=(4,),
+            in_specs=[
+                pl.BlockSpec((chips, step, cols), lambda i, c: (0, i, 0)),
+                pl.BlockSpec((chips, step, cols), lambda i, c: (0, i, 0)),
+                pl.BlockSpec((1, whole), lambda i, c: (0, 0)),
+            ],
+            out_specs=pl.BlockSpec((step, whole), lambda i, c: (i, 0)),
+        ),
+        out_shape=jax.ShapeDtypeStruct((rows, whole), mine.dtype),
+        cost_estimate=pl.CostEstimate(
+            flops=8 * rows * whole, bytes_accessed=4 * rows * whole, transcendentals=rows
+        ),
+    )(core, mine, theirs, gain.reshape(1, whole))
+
+
+def ffn_kernel(core_ref, x_ref, up_ref, down_ref, own_ref, theirs_ref, hid_ref):
+    i = pl.program_id(0)
+    chunk = up_ref.shape[2]
+    ups = hid_ref.shape[1] // chunk
+
+    @pl.when(i < ups)
+    def _():
+        pre = jnp.dot(x_ref[...], up_ref[0], preferred_element_type=jnp.float32)
+        act = jnp.square(jnp.maximum(pre, 0.0)).astype(hid_ref.dtype)
+        hid_ref[:, pl.ds(pl.multiple_of(i * chunk, chunk), chunk)] = act
+
+    @pl.when(i >= ups)
+    def _():
+        both = lax.dot_general(
+            hid_ref[...], down_ref[0, 0], NT, preferred_element_type=jnp.float32
+        ).astype(own_ref.dtype)
+        cols = own_ref.shape[2]
+        first, second = both[:, :cols], both[:, cols:]
+
+        @pl.when(core_ref[0] == 0)
+        def _():
+            own_ref[0] = first
+            theirs_ref[0] = second
+
+        @pl.when(core_ref[0] == 1)
+        def _():
+            own_ref[0] = second
+            theirs_ref[0] = first
+
+
+def ffn_partials(core, x, weights, chips):
+    rows, width = x.shape
+    units = weights.shape[2]
+    cols = width // (2 * chips)
+    chunk = units // 4
+    ups = units // chunk
+    pieces = weights.reshape(2, chips, 2 * cols, units)
+
+    out_spec = pl.BlockSpec((1, rows, cols), lambda i, p: (jnp.maximum(i - ups, 0), 0, 0))
+    return pl.pallas_call(
+        ffn_kernel,
+        grid_spec=pltpu.PrefetchScalarGridSpec(
+            num_scalar_prefetch=1,
+            grid=(ups + chips,),
+            in_specs=[
+                pl.BlockSpec((rows, width), lambda i, p: (0, 0)),
+                pl.BlockSpec((1, width, chunk), lambda i, p: (0, 0, jnp.minimum(i, ups - 1))),
+                pl.BlockSpec((1, 1, 2 * cols, units), lambda i, p: (1, jnp.maximum(i - ups, 0), 0, 0)),
+            ],
+            out_specs=[out_spec, out_spec],
+            scratch_shapes=[pltpu.VMEM((rows, units), x.dtype)],
+        ),
+        out_shape=[jax.ShapeDtypeStruct((chips, rows, cols), x.dtype)] * 2,
+        cost_estimate=pl.CostEstimate(
+            flops=4 * rows * width * units, bytes_accessed=12 << 20, transcendentals=0
+        ),
+    )(core, x, weights, pieces)
+
+
+def sum_at_owners(own, theirs, axis):
+    received = swap_cores(theirs, axis)
+    pair_sum = (own.astype(jnp.float32) + received.astype(jnp.float32)).astype(own.dtype)
+    parts = exchange_chips(pair_sum, axis)
+    return jnp.sum(parts.astype(jnp.float32), axis=0)
 
 
 def per_device(
@@ -117,23 +249,17 @@
     gated_vals = (u_act.astype(jnp.float32) * mixed_vals.reshape(row_count, width)).astype(
         jnp.bfloat16
     )
-    g_mine = gather_chips(gated_vals, "tp")
-    gated_whole = in_order(pair_up(g_mine, swap_cores(g_mine, "tp"), "tp"), 1)
-    mix_vals = jnp.dot(gated_whole, mix, preferred_element_type=jnp.float32)
-    mid_stream = (tokens.astype(jnp.float32) + mix_vals).astype(jnp.bfloat16)
-    cut = row_count // 2
-    m_mine = jnp.concatenate(
-        [gather_chips(mid_stream[:cut], "tp"), gather_chips(mid_stream[cut:], "tp")], 1
-    )
-    mid_whole = in_order(pair_up(m_mine, swap_cores(m_mine, "tp"), "tp"), 1)
-    normed_two = rms_scale(mid_whole.astype(jnp.float32), second_gain).astype(jnp.bfloat16)
-    pre_act = jnp.dot(normed_two, ffn_w[0], preferred_element_type=jnp.float32)
-    hidden_act = jnp.square(jax.nn.relu(pre_act)).astype(jnp.bfloat16)
-    down_terms = lax.dot_general(
-        hidden_act, ffn_w[1], (((1,), (1,)), ((), ())), preferred_element_type=jnp.float32
-    )
-    down_sum = sum_at_owner(down_terms.astype(jnp.bfloat16), "tp", 1)
-    return (mid_stream.astype(jnp.float32) + down_sum).astype(jnp.bfloat16)
+    chips = lax.axis_size("tp") // 2
+    core = jnp.reshape(lax.axis_index("tp") % 2, (1,)).astype(jnp.int32)
+    g_mine = exchange_chips(jnp.broadcast_to(gated_vals, (chips, *gated_vals.shape)), "tp")
+    g_theirs = swap_cores(g_mine, "tp")
+    mid_copies = mix_to_mid(core, g_mine, g_theirs, mix, tokens)
+    m_mine = exchange_chips(mid_copies, "tp")
+    m_theirs = swap_cores(m_mine, "tp")
+    normed_two = norm_pieces(core, m_mine, m_theirs, second_gain)
+    own, theirs = ffn_partials(core, normed_two, ffn_w, chips)
+    down_sum = sum_at_owners(own, theirs, "tp")
+    return (mid_copies[0].astype(jnp.float32) + down_sum).astype(jnp.bfloat16)
 
 
 def solution(mesh):

time: 245 us -> 242 us (0.988)
  blocking collectives: 116 us -> 88 us
  Pallas kernels: 0 us -> 19.6 us
  starting transfers between devices: 70.4 us -> 82.1 us
  matrix products: 9.98 us -> 0.92 us
    all_gather x3 -> x0, blocking collectives: 33.7 us -> none  [gather_chips(): lax.all_gather(x, axis, axis=0, tiled=False, axis_index_groups=[[2 * i +...]
    pallas_call x0 -> x3, Pallas kernels: none -> 19.6 us  [the longest x1 11 us: ffn_partials(): pl.pallas_call(ffn_kernel, grid_spec=pltpu.PrefetchScalarGridSpec(num_sca...]
    ppermute x2 -> x3, starting transfers between devices: 16.3 us -> 28.4 us  [swap_cores(): return lax.ppermute(x, axis, [(i, i ^ 1) for i in range(n)])]
    dot_general x2 -> x0, matrix products: 9.06 us -> none  [the longest x1 8.58 us: per_device(): lax.dot_general(hidden_act, ffn_w[1], (((1,), (1,)), ((), ())), preferred...]
    all_to_all x1 -> x3, blocking collectives: 41.1 us -> 46 us  [exchange_chips(): lax.all_to_all(blocks, axis, split_axis=0, concat_axis=0, tiled=True, axi...]
    convert_element_type x1 -> x0, local copies, waits for them, and re-layouts: 2.47 us -> none  [per_device(): rms_scale(mid_whole.astype(jnp.float32), second_gain).astype(jnp.bfloat16)]
    unnamed x22 -> x28, local copies, waits for them, and re-layouts: 3.62 us -> 5.14 us
  transfers between devices with their start and end apart: 6 -> 7, of which waited for: 4 -> 4; matrix products, arithmetic and copies ran while one was open for 6% -> 4% of each run, Pallas kernels for 0% -> 4%
where the time goes in v2:
time: 242 us; the launch traced here: 241 us
  blocking collectives  88 us (36%)
  starting transfers between devices  82.1 us (34%)
  Pallas kernels  19.6 us (8%)
  waiting for transfers between devices  19 us (8%)
  between operations  13.7 us (6%)
  local copies, waits for them, and re-layouts  10.4 us (4%)
  other arithmetic  6.9 us (3%)
    all_to_all x3, blocking collectives, exchange_chips(): lax.all_to_all(blocks, axis, split_axis=0, concat_axis=0, tiled=True, axi...  46 us
    all_to_all x1, starting transfers between devices, sent_to_all(): return lax.all_to_all(copies, axis, split_axis=0, concat_axis=0, tiled=True)  45.1 us
    all_gather x1, blocking collectives, gather_two_level(): lax.all_gather(shard, axis, axis=0, tiled=False, axis_index_groups=[[r +...  41.9 us
    ppermute x3, starting transfers between devices, swap_cores(): return lax.ppermute(x, axis, [(i, i ^ 1) for i in range(n)])  28.4 us
    ppermute x2, waiting for transfers between devices, shift(): return lax.ppermute(x, axis, [(i, (i + by) % n) for i in range(n)])  14.8 us
    pallas_call x1, Pallas kernels, ffn_partials(): pl.pallas_call(ffn_kernel, grid_spec=pltpu.PrefetchScalarGridSpec(num_sca...  11 us
    ppermute x2, starting transfers between devices, shift(): return lax.ppermute(x, axis, [(i, (i + by) % n) for i in range(n)])  8.61 us
    unnamed x28, local copies, waits for them, and re-layouts  5.14 us
  transfers between devices with their start and end apart: 7, of which 4 were waited for; matrix products, arithmetic and copies ran while one was open for 4% of the time, Pallas kernels for 4%

profile of v2, /device:TPU:33, one launch (start us, length us, event | category | flops | bytes accessed | tf_op | source)
XLA Modules:
  0.0 240.6 jit_solution(3119584065551083930)
XLA Ops:
  6.6 1.7 pad_maximum_fusion.1
  8.3 1.1 copy.13
  9.4 1.6 broadcast_in_dim.7
  11.0 45.1 %all-to-all-start = ((bf16[8,512,256]{1,2,0:T(8,128)(2,1)}), bf16[8,512,256]{1,2,0:T(8,128)(2,1)S(1)}, u32[]{:S(2)}, u32[]{:S(2)}) async-start(bf16[8,512,256]{1,2,0:T(8,128)(2,1)} %broadcast_in_dim.7), calls=%async_computation | async-start | bytes 4194304 | tf_op jit(solution)/shard_map/all_to_all | solution.py:18
  56.1 41.9 %all-gather = bf16[1536,256]{1,0:T(8,128)(2,1)S(1)} all-gather(bf16[96,256]{1,0:T(8,128)(2,1)S(1)} %pad_maximum_fusion.2), channel_id=2, replica_groups={{0,16,32,48,64,80,96,112,128,144,160,176,192,208,224,240},{8,24,40,56,7..., dimensions={0}, use_global_device_ids=true | all-gather | bytes 835584 | tf_op jit(solution)/shard_map/all_gather | solution.py:35
  98.1 0.9 fusion.26
  99.0 6.7 %collective-permute-start = (bf16[8,96,256]{2,1,0:T(8,128)(2,1)}, bf16[8,96,256]{2,1,0:T(8,128)(2,1)}, u32[]{:S(2)}, u32[]{:S(2)}) collective-permute-start(bf16[8,96,256]{2,1,0:T(8,128)(2,1)} %bitcast.3), channel_id=1, source_target_pairs={{0,8},{8,16},{16,24},{24,32},{32,40},{40,48},{48,56},{56,64},{64,7... | collective-permute-start | bytes 1179656 | tf_op jit(solution)/shard_map/ppermute | solution.py:29
  105.7 2.0 collective-permute-start.1
  107.7 12.2 %collective-permute-done = bf16[8,96,256]{2,1,0:T(8,128)(2,1)} collective-permute-done((bf16[8,96,256]{2,1,0:T(8,128)(2,1)}, bf16[8,96,256]{2,1,0:T(8,128)(2,1)}, u32[]{:S(2)}, u32[]{:S(2)}) %collective-permute-start) | collective-permute-done | bytes 393248 | tf_op jit(solution)/shard_map/ppermute | solution.py:29
  119.9 1.0 constant_dynamic-update-slice_fusion.1
  120.9 2.6 %collective-permute-done.1 = bf16[8,96,256]{2,1,0:T(8,128)(2,1)S(1)} collective-permute-done((bf16[8,96,256]{2,1,0:T(8,128)(2,1)}, bf16[8,96,256]{2,1,0:T(8,128)(2,1)S(1)}, u32[]{:S(2)}, u32[]{:S(2)}) %collective-permute-start.1) | collective-permute-done | bytes 393248 | tf_op jit(solution)/shard_map/ppermute | solution.py:29
  124.0 1.1 copy-done
  125.3 0.5 fusion
  125.8 0.5 fusion.2
  126.3 0.7 fusion.27
  127.8 9.4 %all_to_all.20.mine_ref = bf16[4,512,128]{2,1,0:T(8,128)(2,1)S(1)} all-to-all(bf16[4,512,128]{2,1,0:T(8,128)(2,1)S(1)} %broadcast_in_dim.10), channel_id=1, replica_groups={{0,2,4,6},{1,3,5,7},{8,10,12,14},{9,11,13,15},{16,18,20,22},{17,19,21,2..., dimensions={0} | all-to-all | bytes 1048576 | tf_op jit(solution)/shard_map/all_to_all | solution.py:60
  137.2 10.2 %collective-permute-start.2 = (bf16[4,512,128]{2,1,0:T(8,128)(2,1)S(1)}, bf16[4,512,128]{2,1,0:T(8,128)(2,1)S(1)}, u32[]{:S(2)}, u32[]{:S(2)}) collective-permute-start(bf16[4,512,128]{2,1,0:T(8,128)(2,1)S(1)} %all_to_all.20.mine_ref), channel_id=1, source_target_pairs={{0,1},{1,0},{2,3},{3,2},{4,5},{5,4},{6,7},{7,6},{8,9},{9,8},{10,11... | collective-permute-start | bytes 1572872 | tf_op jit(solution)/shard_map/ppermute | solution.py:51
  147.4 1.9 slice.35
  149.4 0.8 copy-done.4
  150.2 4.2 %shard_map.109 = bf16[4,512,256]{2,1,0:T(8,128)(2,1)} custom-call(s32[1]{0:T(128)} %bitcast.core_ref, bf16[4,512,128]{2,1,0:T(8,128)(2,1)} %copy-done.2, bf16[4,512,128]{2,1,0:T(8,128)(2,1)} %copy-done.4, bf16[8,128,256]{2,1,0:T(8,128)(2,1)} %bitcast.54, bf16[512,256]{1,0:T(8,128)(2,1)} %tok_ref.1), custom_call_target="tpu_custom_call" | custom-call | flops 268435456 | bytes 4194304 | tf_op jit(solution)/shard_map/pallas_call | solution.py:87
  154.4 18.4 %all_to_all.21.mine_ref = bf16[4,512,256]{2,1,0:T(8,128)(2,1)S(1)} all-to-all(bf16[4,512,256]{2,1,0:T(8,128)(2,1)} %shard_map.109), channel_id=1, replica_groups={{0,2,4,6},{1,3,5,7},{8,10,12,14},{9,11,13,15},{16,18,20,22},{17,19,21,2..., dimensions={0} | all-to-all | bytes 2097152 | tf_op jit(solution)/shard_map/all_to_all | solution.py:60
  172.8 3.1 %collective-permute-start.3 = (bf16[4,512,256]{2,1,0:T(8,128)(2,1)S(1)}, bf16[4,512,256]{2,1,0:T(8,128)(2,1)S(1)}, u32[]{:S(2)}, u32[]{:S(2)}) collective-permute-start(bf16[4,512,256]{2,1,0:T(8,128)(2,1)S(1)} %all_to_all.21.mine_ref), channel_id=1, source_target_pairs={{0,1},{1,0},{2,3},{3,2},{4,5},{5,4},{6,7},{7,6},{8,9},{9,8},{10,11... | collective-permute-start | bytes 3145736 | tf_op jit(solution)/shard_map/ppermute | solution.py:51
  175.9 0.6 reshape.95.gain_ref
  176.5 1.7 collective-permute-done.3.theirs_ref
  178.2 1.0 copy-done.3
  179.2 4.4 %shard_map.110.x_ref = bf16[512,2048]{1,0:T(8,128)(2,1)} custom-call(s32[1]{0:T(128)} %bitcast.core_ref, bf16[4,512,256]{2,1,0:T(8,128)(2,1)} %copy-done.1, bf16[4,512,256]{2,1,0:T(8,128)(2,1)} %copy-done.3, bf16[1,2048]{1,0:T(2,128)(2,1)} %reshape.95.gain_ref), custom_call_target="tpu_custom_call" | custom-call | flops 8388608 | bytes 4194304 | tf_op jit(solution)/shard_map/pallas_call | solution.py:127
  183.6 11.0 %shard_map.111 = (bf16[4,512,256]{2,1,0:T(8,128)(2,1)}, bf16[4,512,256]{2,1,0:T(8,128)(2,1)}) custom-call(s32[1]{0:T(128)} %bitcast.core_ref, bf16[512,2048]{1,0:T(8,128)(2,1)} %shard_map.110.x_ref, bf16[2,2048,1024]{2,1,0:T(8,128)(2,1)} %all-gather.3.cloned.1.call-done.up_ref, bf16[2,4,512,1024]{3,2,1,0:T(8,128)(2,1)} %bitcast.48), custom_call_target="tpu_custom_call" | custom-call | flops 4294967296 | bytes 12582912 | tf_op jit(solution)/shard_map/pallas_call | solution.py:185
  194.6 15.1 %collective-permute-start.4 = (bf16[4,512,256]{2,1,0:T(8,128)(2,1)}, bf16[4,512,256]{2,1,0:T(8,128)(2,1)S(1)}, u32[]{:S(2)}, u32[]{:S(2)}) collective-permute-start(bf16[4,512,256]{2,1,0:T(8,128)(2,1)} %get-tuple-element.8), channel_id=1, source_target_pairs={{0,1},{1,0},{2,3},{3,2},{4,5},{5,4},{6,7},{7,6},{8,9},{9,8},{10,11... | collective-permute-start | bytes 3145736 | tf_op jit(solution)/shard_map/ppermute | solution.py:51
  209.7 2.5 %collective-permute-done.4 = bf16[4,512,256]{2,1,0:T(8,128)(2,1)S(1)} collective-permute-done((bf16[4,512,256]{2,1,0:T(8,128)(2,1)}, bf16[4,512,256]{2,1,0:T(8,128)(2,1)S(1)}, u32[]{:S(2)}, u32[]{:S(2)}) %collective-permute-start.4) | collective-permute-done | bytes 1048608 | tf_op jit(solution)/shard_map/ppermute | solution.py:51
  212.2 1.5 add_convert_fusion
  213.7 18.2 %all_to_all.22 = bf16[4,512,256]{2,1,0:T(8,128)(2,1)S(1)} all-to-all(bf16[4,512,256]{2,1,0:T(8,128)(2,1)S(1)} %add_convert_fusion), channel_id=1, replica_groups={{0,2,4,6},{1,3,5,7},{8,10,12,14},{9,11,13,15},{16,18,20,22},{17,19,21,2..., dimensions={0} | all-to-all | bytes 2097152 | tf_op jit(solution)/shard_map/all_to_all | solution.py:60
  232.1 1.7 fusion.4
  (45 shorter events, 1.5 us)
Async XLA Ops:
  6.5 177.1 %all-gather.3.cloned.1.call-start = ((), (), s32[]{:S(2)}) async-start(), calls=%async_computation.4 | async-start | bytes 8650752 | tf_op jit(solution)/shard_map/all_gather | solution.py:225
  11.0 45.1 %copy-start.6 = (bf16[32,256]{1,0:T(8,128)(2,1)S(1)}, bf16[32,256]{1,0:T(8,128)(2,1)}, u32[]{:S(2)}) copy-start(bf16[32,256]{1,0:T(8,128)(2,1)} %param.18) | copy-start | bytes 49156
  11.0 45.1 %copy-start.7 = (bf16[64,128]{1,0:T(8,128)(2,1)S(1)}, bf16[64,128]{1,0:T(8,128)(2,1)}, u32[]{:S(2)}) copy-start(bf16[64,128]{1,0:T(8,128)(2,1)} %param.14) | copy-start | bytes 49156
  11.0 45.1 %copy-start.8 = (bf16[64,128]{1,0:T(8,128)(2,1)S(1)}, bf16[64,128]{1,0:T(8,128)(2,1)}, u32[]{:S(2)}) copy-start(bf16[64,128]{1,0:T(8,128)(2,1)} %param.13) | copy-start | bytes 49156
  11.0 114.3 %all-to-all-start = ((bf16[8,512,256]{1,2,0:T(8,128)(2,1)}), bf16[8,512,256]{1,2,0:T(8,128)(2,1)S(1)}, u32[]{:S(2)}, u32[]{:S(2)}) async-start(bf16[8,512,256]{1,2,0:T(8,128)(2,1)} %broadcast_in_dim.7), calls=%async_computation | async-start | bytes 4194304 | tf_op jit(solution)/shard_map/all_to_all | solution.py:18
  56.1 51.6 %copy-start.11 = (bf16[1,128]{1,0:T(2,128)(2,1)S(1)}, bf16[1,128]{1,0:T(2,128)(2,1)}, u32[]{:S(2)}) copy-start(bf16[1,128]{1,0:T(2,128)(2,1)} %param.15) | copy-start | bytes 772
  56.1 51.6 %copy-start.9 = (bf16[2048]{0:T(1024)(128)(2,1)S(1)}, bf16[2048]{0:T(1024)(128)(2,1)}, u32[]{:S(2)}) copy-start(bf16[2048]{0:T(1024)(128)(2,1)} %param.12) | copy-start | bytes 12292
  56.1 51.6 %copy-start.12 = (bf16[1,128]{1,0:T(2,128)(2,1)S(1)}, bf16[1,128]{1,0:T(2,128)(2,1)}, u32[]{:S(2)}) copy-start(bf16[1,128]{1,0:T(2,128)(2,1)} %param.17) | copy-start | bytes 772
  99.0 20.9 %collective-permute-start = (bf16[8,96,256]{2,1,0:T(8,128)(2,1)}, bf16[8,96,256]{2,1,0:T(8,128)(2,1)}, u32[]{:S(2)}, u32[]{:S(2)}) collective-permute-start(bf16[8,96,256]{2,1,0:T(8,128)(2,1)} %bitcast.3), channel_id=1, source_target_pairs={{0,8},{8,16},{16,24},{24,32},{32,40},{40,48},{48,56},{56,64},{64,7... | collective-permute-start | bytes 1179656 | tf_op jit(solution)/shard_map/ppermute | solution.py:29
  105.7 17.8 %collective-permute-start.1 = (bf16[8,96,256]{2,1,0:T(8,128)(2,1)}, bf16[8,96,256]{2,1,0:T(8,128)(2,1)S(1)}, u32[]{:S(2)}, u32[]{:S(2)}) collective-permute-start(bf16[8,96,256]{2,1,0:T(8,128)(2,1)} %bitcast.4), channel_id=1, source_target_pairs={{0,248},{8,0},{16,8},{24,16},{32,24},{40,32},{48,40},{56,48},{64,5... | collective-permute-start | bytes 1179656 | tf_op jit(solution)/shard_map/ppermute | solution.py:29
  124.0 1.1 copy-start
  126.3 1.1 copy-start.5
  137.2 12.1 %copy-start.2 = (bf16[4,512,128]{2,1,0:T(8,128)(2,1)}, bf16[4,512,128]{2,1,0:T(8,128)(2,1)S(1)}, u32[]{:S(2)}) copy-start(bf16[4,512,128]{2,1,0:T(8,128)(2,1)S(1)} %all_to_all.20.mine_ref) | copy-start | bytes 1572868
  137.2 12.1 %collective-permute-start.2 = (bf16[4,512,128]{2,1,0:T(8,128)(2,1)S(1)}, bf16[4,512,128]{2,1,0:T(8,128)(2,1)S(1)}, u32[]{:S(2)}, u32[]{:S(2)}) collective-permute-start(bf16[4,512,128]{2,1,0:T(8,128)(2,1)S(1)} %all_to_all.20.mine_ref), channel_id=1, source_target_pairs={{0,1},{1,0},{2,3},{3,2},{4,5},{5,4},{6,7},{7,6},{8,9},{9,8},{10,11... | collective-permute-start | bytes 1572872 | tf_op jit(solution)/shard_map/ppermute | solution.py:51
  149.4 0.8 copy-start.4
  150.2 25.7 %copy-start.10 = (bf16[2048]{0:T(1024)(128)(2,1)S(1)}, bf16[2048]{0:T(1024)(128)(2,1)}, u32[]{:S(2)}) copy-start(bf16[2048]{0:T(1024)(128)(2,1)} %param.19) | copy-start | bytes 12292
  172.8 5.4 %copy-start.1 = (bf16[4,512,256]{2,1,0:T(8,128)(2,1)}, bf16[4,512,256]{2,1,0:T(8,128)(2,1)S(1)}, u32[]{:S(2)}) copy-start(bf16[4,512,256]{2,1,0:T(8,128)(2,1)S(1)} %all_to_all.21.mine_ref) | copy-start | bytes 3145732
  172.8 5.4 %collective-permute-start.3 = (bf16[4,512,256]{2,1,0:T(8,128)(2,1)S(1)}, bf16[4,512,256]{2,1,0:T(8,128)(2,1)S(1)}, u32[]{:S(2)}, u32[]{:S(2)}) collective-permute-start(bf16[4,512,256]{2,1,0:T(8,128)(2,1)S(1)} %all_to_all.21.mine_ref), channel_id=1, source_target_pairs={{0,1},{1,0},{2,3},{3,2},{4,5},{5,4},{6,7},{7,6},{8,9},{9,8},{10,11... | collective-permute-start | bytes 3145736 | tf_op jit(solution)/shard_map/ppermute | solution.py:51
  178.2 1.0 copy-start.3
  194.6 17.6 %collective-permute-start.4 = (bf16[4,512,256]{2,1,0:T(8,128)(2,1)}, bf16[4,512,256]{2,1,0:T(8,128)(2,1)S(1)}, u32[]{:S(2)}, u32[]{:S(2)}) collective-permute-start(bf16[4,512,256]{2,1,0:T(8,128)(2,1)} %get-tuple-element.8), channel_id=1, source_target_pairs={{0,1},{1,0},{2,3},{3,2},{4,5},{5,4},{6,7},{7,6},{8,9},{9,8},{10,11... | collective-permute-start | bytes 3145736 | tf_op jit(solution)/shard_map/ppermute | solution.py:51
Sparse Core Ops, SparseCore 0:
  9.4 172.9 all-gather.2

commit v3 on v2

--- a/solution.py
+++ b/solution.py
@@ -29,13 +29,28 @@
     return lax.ppermute(x, axis, [(i, (i + by) % n) for i in range(n)])
 
 
-def gather_two_level(shard, axis):
+def own_parity(shard, axis):
+    n = lax.axis_size(axis)
+    return lax.all_gather(
+        shard, axis, axis=0, tiled=False,
+        axis_index_groups=[[r + 2 * i for i in range(n // 2)] for r in range(2)],
+    )
+
+
+def gather_two_level(shard, axis, twin_axis):
     n = lax.axis_size(axis)
     half = n // 2
-    own = lax.all_gather(
-        shard, axis, axis=0, tiled=False,
-        axis_index_groups=[[r + 2 * i for i in range(half)] for r in range(2)],
-    )
+    twins = lax.axis_size(twin_axis)
+    if twins % 2 == 0:
+        rows = shard.shape[0] // 2
+        upper = lax.axis_index(twin_axis) % 2 == 1
+        mine = own_parity(jnp.where(upper, shard[rows:], shard[:rows]), axis)
+        theirs = lax.ppermute(mine, twin_axis, [(i, i ^ 1) for i in range(twins)])
+        own = jnp.concatenate(
+            [jnp.where(upper, theirs, mine), jnp.where(upper, mine, theirs)], 1
+        )
+    else:
+        own = own_parity(shard, axis)
     cut = half // 2
     from_left = shift(own[:cut], axis, 1)
     from_right = shift(own[cut:], axis, -1)
@@ -225,7 +240,7 @@
     ffn_w = lax.all_gather(jnp.stack([up_proj, down_proj.T]), "fs", axis=1, tiled=True)
     whole_rows = in_order(sent_to_all(tokens, "tp"), 1)
     small = jnp.concatenate([jnp.concatenate([u_proj, v_proj], 1), mix_proj], 0)
-    small_all = gather_two_level(small, "fs")
+    small_all = gather_two_level(small, "fs", "grp")
     rows_uv = u_proj.shape[0]
     width = u_proj.shape[1]
     uv = small_all[:, :rows_uv].reshape(-1, 2 * width)

time: 242 us -> 237 us (0.979)
  blocking collectives: 88 us -> 81.2 us
  waiting for transfers between devices: 19 us -> 22.5 us
    all_gather x1, blocking collectives: 41.9 us -> 33.6 us  [own_parity(): lax.all_gather(shard, axis, axis=0, tiled=False, axis_index_groups=[[r +...]
    ppermute x0 -> x1, waiting for transfers between devices: none -> 5.51 us  [gather_two_level(): theirs = lax.ppermute(mine, twin_axis, [(i, i ^ 1) for i in range(twins)])]
    ppermute x0 -> x1, starting transfers between devices: none -> 3.99 us  [gather_two_level(): theirs = lax.ppermute(mine, twin_axis, [(i, i ^ 1) for i in range(twins)])]
  transfers between devices with their start and end apart: 7 -> 8, of which waited for: 4 -> 5; matrix products, arithmetic and copies ran while one was open for 4% -> 4% of each run, Pallas kernels for 4% -> 4%
where the time goes in v3:
time: 237 us; the launch traced here: 236 us
  starting transfers between devices  82.7 us (35%)
  blocking collectives  81.2 us (34%)
  waiting for transfers between devices  22.5 us (9%)
  Pallas kernels  19.6 us (8%)
  between operations  13.7 us (6%)
  local copies, waits for them, and re-layouts  8.44 us (4%)
  other arithmetic  7.18 us (3%)
    all_to_all x3, blocking collectives, exchange_chips(): lax.all_to_all(blocks, axis, split_axis=0, concat_axis=0, tiled=True, axi...  47.6 us
    all_to_all x1, starting transfers between devices, sent_to_all(): return lax.all_to_all(copies, axis, split_axis=0, concat_axis=0, tiled=True)  45.1 us
    all_gather x1, blocking collectives, own_parity(): lax.all_gather(shard, axis, axis=0, tiled=False, axis_index_groups=[[r +...  33.6 us
    ppermute x3, starting transfers between devices, swap_cores(): return lax.ppermute(x, axis, [(i, i ^ 1) for i in range(n)])  27 us
    ppermute x2, waiting for transfers between devices, shift(): return lax.ppermute(x, axis, [(i, (i + by) % n) for i in range(n)])  12.8 us
    pallas_call x1, Pallas kernels, ffn_partials(): pl.pallas_call(ffn_kernel, grid_spec=pltpu.PrefetchScalarGridSpec(num_sca...  11 us
    ppermute x2, starting transfers between devices, shift(): return lax.ppermute(x, axis, [(i, (i + by) % n) for i in range(n)])  6.55 us
    ppermute x1, waiting for transfers between devices, gather_two_level(): theirs = lax.ppermute(mine, twin_axis, [(i, i ^ 1) for i in range(twins)])  5.51 us
  transfers between devices with their start and end apart: 8, of which 5 were waited for; matrix products, arithmetic and copies ran while one was open for 4% of the time, Pallas kernels for 4%

profile of v3, /device:TPU:33, one launch (start us, length us, event | category | flops | bytes accessed | tf_op | source)
XLA Modules:
  0.0 236.3 jit_solution(7840503072452504543)
XLA Ops:
  6.6 1.7 pad_maximum_fusion.4
  8.3 1.1 copy.13
  9.4 1.6 broadcast_in_dim.7
  11.0 45.1 %all-to-all-start = ((bf16[8,512,256]{1,2,0:T(8,128)(2,1)}), bf16[8,512,256]{1,2,0:T(8,128)(2,1)S(1)}, u32[]{:S(2)}, u32[]{:S(2)}) async-start(bf16[8,512,256]{1,2,0:T(8,128)(2,1)} %broadcast_in_dim.7), calls=%async_computation | async-start | bytes 4194304 | tf_op jit(solution)/shard_map/all_to_all | solution.py:18
  56.2 33.6 %all-gather = bf16[768,256]{1,0:T(8,128)(2,1)S(1)} all-gather(bf16[48,256]{1,0:T(8,128)(2,1)S(1)} %slice_select_fusion), channel_id=2, replica_groups={{0,16,32,48,64,80,96,112,128,144,160,176,192,208,224,240},{8,24,40,56,7..., dimensions={0}, use_global_device_ids=true | all-gather | bytes 417792 | tf_op jit(solution)/shard_map/all_gather | solution.py:34
  89.8 4.0 %collective-permute-start = (bf16[16,48,256]{2,1,0:T(8,128)(2,1)S(1)}, bf16[16,48,256]{2,1,0:T(8,128)(2,1)S(1)}, u32[]{:S(2)}, u32[]{:S(2)}) collective-permute-start(bf16[16,48,256]{2,1,0:T(8,128)(2,1)S(1)} %bitcast.54), channel_id=1, source_target_pairs={{0,256},{256,0},{1,257},{257,1},{2,258},{258,2},{3,259},{259,3},{4... | collective-permute-start | bytes 1179656 | tf_op jit(solution)/shard_map/ppermute | solution.py:48
  93.8 5.5 %collective-permute-done = bf16[16,48,256]{2,1,0:T(8,128)(2,1)S(1)} collective-permute-done((bf16[16,48,256]{2,1,0:T(8,128)(2,1)S(1)}, bf16[16,48,256]{2,1,0:T(8,128)(2,1)S(1)}, u32[]{:S(2)}, u32[]{:S(2)}) %collective-permute-start) | collective-permute-done | bytes 393248 | tf_op jit(solution)/shard_map/ppermute | solution.py:48
  99.5 3.3 %collective-permute-start.1 = (bf16[8,96,256]{2,1,0:T(8,128)(2,1)S(1)}, bf16[8,96,256]{2,1,0:T(8,128)(2,1)S(1)}, u32[]{:S(2)}, u32[]{:S(2)}) collective-permute-start(bf16[8,96,256]{2,1,0:T(8,128)(2,1)S(1)} %get-tuple-element.11), channel_id=1, source_target_pairs={{0,8},{8,16},{16,24},{24,32},{32,40},{40,48},{48,56},{56,64},{64,7... | collective-permute-start | bytes 1179656 | tf_op jit(solution)/shard_map/ppermute | solution.py:29
  102.8 3.2 %collective-permute-start.2 = (bf16[8,96,256]{2,1,0:T(8,128)(2,1)S(1)}, bf16[8,96,256]{2,1,0:T(8,128)(2,1)S(1)}, u32[]{:S(2)}, u32[]{:S(2)}) collective-permute-start(bf16[8,96,256]{2,1,0:T(8,128)(2,1)S(1)} %get-tuple-element.12), channel_id=1, source_target_pairs={{0,248},{8,0},{16,8},{24,16},{32,24},{40,32},{48,40},{56,48},{64,5... | collective-permute-start | bytes 1179656 | tf_op jit(solution)/shard_map/ppermute | solution.py:29
  106.1 12.7 %collective-permute-done.1 = bf16[8,96,256]{2,1,0:T(8,128)(2,1)S(1)} collective-permute-done((bf16[8,96,256]{2,1,0:T(8,128)(2,1)S(1)}, bf16[8,96,256]{2,1,0:T(8,128)(2,1)S(1)}, u32[]{:S(2)}, u32[]{:S(2)}) %collective-permute-start.1) | collective-permute-done | bytes 393248 | tf_op jit(solution)/shard_map/ppermute | solution.py:29
  118.9 0.4 broadcast_select_fusion.1
  119.6 1.1 copy-done
  120.8 0.5 fusion
  121.3 0.5 fusion.2
  121.8 0.7 fusion.27
  123.3 11.5 %all_to_all.20.mine_ref = bf16[4,512,128]{2,1,0:T(8,128)(2,1)S(1)} all-to-all(bf16[4,512,128]{2,1,0:T(8,128)(2,1)S(1)} %broadcast_in_dim.10), channel_id=1, replica_groups={{0,2,4,6},{1,3,5,7},{8,10,12,14},{9,11,13,15},{16,18,20,22},{17,19,21,2..., dimensions={0} | all-to-all | bytes 1048576 | tf_op jit(solution)/shard_map/all_to_all | solution.py:75
  134.8 12.2 %collective-permute-start.3 = (bf16[4,512,128]{2,1,0:T(8,128)(2,1)S(1)}, bf16[4,512,128]{2,1,0:T(8,128)(2,1)S(1)}, u32[]{:S(2)}, u32[]{:S(2)}) collective-permute-start(bf16[4,512,128]{2,1,0:T(8,128)(2,1)S(1)} %all_to_all.20.mine_ref), channel_id=1, source_target_pairs={{0,1},{1,0},{2,3},{3,2},{4,5},{5,4},{6,7},{7,6},{8,9},{9,8},{10,11... | collective-permute-start | bytes 1572872 | tf_op jit(solution)/shard_map/ppermute | solution.py:66
  147.0 1.9 slice.42
  148.9 0.8 copy-done.4
  149.7 4.2 %shard_map.109 = bf16[4,512,256]{2,1,0:T(8,128)(2,1)} custom-call(s32[1]{0:T(128)} %bitcast.core_ref, bf16[4,512,128]{2,1,0:T(8,128)(2,1)} %copy-done.2, bf16[4,512,128]{2,1,0:T(8,128)(2,1)} %copy-done.4, bf16[8,128,256]{2,1,0:T(8,128)(2,1)} %bitcast.53, bf16[512,256]{1,0:T(8,128)(2,1)} %tok_ref.1), custom_call_target="tpu_custom_call" | custom-call | flops 268435456 | bytes 4194304 | tf_op jit(solution)/shard_map/pallas_call | solution.py:102
  153.9 18.5 %all_to_all.21.mine_ref = bf16[4,512,256]{2,1,0:T(8,128)(2,1)S(1)} all-to-all(bf16[4,512,256]{2,1,0:T(8,128)(2,1)} %shard_map.109), channel_id=1, replica_groups={{0,2,4,6},{1,3,5,7},{8,10,12,14},{9,11,13,15},{16,18,20,22},{17,19,21,2..., dimensions={0} | all-to-all | bytes 2097152 | tf_op jit(solution)/shard_map/all_to_all | solution.py:75
  172.4 3.0 %collective-permute-start.4 = (bf16[4,512,256]{2,1,0:T(8,128)(2,1)S(1)}, bf16[4,512,256]{2,1,0:T(8,128)(2,1)S(1)}, u32[]{:S(2)}, u32[]{:S(2)}) collective-permute-start(bf16[4,512,256]{2,1,0:T(8,128)(2,1)S(1)} %all_to_all.21.mine_ref), channel_id=1, source_target_pairs={{0,1},{1,0},{2,3},{3,2},{4,5},{5,4},{6,7},{7,6},{8,9},{9,8},{10,11... | collective-permute-start | bytes 3145736 | tf_op jit(solution)/shard_map/ppermute | solution.py:66
  175.4 0.6 reshape.205.gain_ref
  176.0 1.7 collective-permute-done.4.theirs_ref
  177.7 1.0 copy-done.3
  178.7 4.4 %shard_map.110.x_ref = bf16[512,2048]{1,0:T(8,128)(2,1)} custom-call(s32[1]{0:T(128)} %bitcast.core_ref, bf16[4,512,256]{2,1,0:T(8,128)(2,1)} %copy-done.1, bf16[4,512,256]{2,1,0:T(8,128)(2,1)} %copy-done.3, bf16[1,2048]{1,0:T(2,128)(2,1)} %reshape.205.gain_ref), custom_call_target="tpu_custom_call" | custom-call | flops 8388608 | bytes 4194304 | tf_op jit(solution)/shard_map/pallas_call | solution.py:142
  183.1 11.0 %shard_map.111 = (bf16[4,512,256]{2,1,0:T(8,128)(2,1)}, bf16[4,512,256]{2,1,0:T(8,128)(2,1)}) custom-call(s32[1]{0:T(128)} %bitcast.core_ref, bf16[512,2048]{1,0:T(8,128)(2,1)} %shard_map.110.x_ref, bf16[2,2048,1024]{2,1,0:T(8,128)(2,1)} %all-gather.3.cloned.1.call-done.up_ref, bf16[2,4,512,1024]{3,2,1,0:T(8,128)(2,1)} %bitcast.46), custom_call_target="tpu_custom_call" | custom-call | flops 4294967296 | bytes 12582912 | tf_op jit(solution)/shard_map/pallas_call | solution.py:200
  194.1 11.8 %collective-permute-start.5 = (bf16[4,512,256]{2,1,0:T(8,128)(2,1)}, bf16[4,512,256]{2,1,0:T(8,128)(2,1)S(1)}, u32[]{:S(2)}, u32[]{:S(2)}) collective-permute-start(bf16[4,512,256]{2,1,0:T(8,128)(2,1)} %get-tuple-element.8), channel_id=1, source_target_pairs={{0,1},{1,0},{2,3},{3,2},{4,5},{5,4},{6,7},{7,6},{8,9},{9,8},{10,11... | collective-permute-start | bytes 3145736 | tf_op jit(solution)/shard_map/ppermute | solution.py:66
  205.9 2.5 %collective-permute-done.5 = bf16[4,512,256]{2,1,0:T(8,128)(2,1)S(1)} collective-permute-done((bf16[4,512,256]{2,1,0:T(8,128)(2,1)}, bf16[4,512,256]{2,1,0:T(8,128)(2,1)S(1)}, u32[]{:S(2)}, u32[]{:S(2)}) %collective-permute-start.5) | collective-permute-done | bytes 1048608 | tf_op jit(solution)/shard_map/ppermute | solution.py:66
  208.4 1.5 add_convert_fusion
  209.9 17.6 %all_to_all.22 = bf16[4,512,256]{2,1,0:T(8,128)(2,1)S(1)} all-to-all(bf16[4,512,256]{2,1,0:T(8,128)(2,1)S(1)} %add_convert_fusion), channel_id=1, replica_groups={{0,2,4,6},{1,3,5,7},{8,10,12,14},{9,11,13,15},{16,18,20,22},{17,19,21,2..., dimensions={0} | all-to-all | bytes 2097152 | tf_op jit(solution)/shard_map/all_to_all | solution.py:75
  227.7 1.7 fusion.4
  (48 shorter events, 1.5 us)
Async XLA Ops:
  6.5 176.6 %all-gather.3.cloned.1.call-start = ((), (), s32[]{:S(2)}) async-start(), calls=%async_computation.4 | async-start | bytes 8650752 | tf_op jit(solution)/shard_map/all_gather | solution.py:240
  11.0 45.1 %copy-start.6 = (bf16[64,128]{1,0:T(8,128)(2,1)S(1)}, bf16[64,128]{1,0:T(8,128)(2,1)}, u32[]{:S(2)}) copy-start(bf16[64,128]{1,0:T(8,128)(2,1)} %param.13) | copy-start | bytes 49156
  11.0 45.1 %copy-start.7 = (bf16[64,128]{1,0:T(8,128)(2,1)S(1)}, bf16[64,128]{1,0:T(8,128)(2,1)}, u32[]{:S(2)}) copy-start(bf16[64,128]{1,0:T(8,128)(2,1)} %param.14) | copy-start | bytes 49156
  11.0 45.1 %copy-start.8 = (bf16[32,256]{1,0:T(8,128)(2,1)S(1)}, bf16[32,256]{1,0:T(8,128)(2,1)}, u32[]{:S(2)}) copy-start(bf16[32,256]{1,0:T(8,128)(2,1)} %param.18) | copy-start | bytes 49156
  11.0 82.8 %copy-start.9 = (bf16[2048]{0:T(1024)(128)(2,1)S(1)}, bf16[2048]{0:T(1024)(128)(2,1)}, u32[]{:S(2)}) copy-start(bf16[2048]{0:T(1024)(128)(2,1)} %param.12) | copy-start | bytes 12292
  11.0 109.8 %all-to-all-start = ((bf16[8,512,256]{1,2,0:T(8,128)(2,1)}), bf16[8,512,256]{1,2,0:T(8,128)(2,1)S(1)}, u32[]{:S(2)}, u32[]{:S(2)}) async-start(bf16[8,512,256]{1,2,0:T(8,128)(2,1)} %broadcast_in_dim.7), calls=%async_computation | async-start | bytes 4194304 | tf_op jit(solution)/shard_map/all_to_all | solution.py:18
  56.1 50.0 %copy-start.11 = (bf16[1,128]{1,0:T(2,128)(2,1)S(1)}, bf16[1,128]{1,0:T(2,128)(2,1)}, u32[]{:S(2)}) copy-start(bf16[1,128]{1,0:T(2,128)(2,1)} %param.15) | copy-start | bytes 772
  56.1 50.0 %copy-start.12 = (bf16[1,128]{1,0:T(2,128)(2,1)S(1)}, bf16[1,128]{1,0:T(2,128)(2,1)}, u32[]{:S(2)}) copy-start(bf16[1,128]{1,0:T(2,128)(2,1)} %param.17) | copy-start | bytes 772
  89.8 9.6 %collective-permute-start = (bf16[16,48,256]{2,1,0:T(8,128)(2,1)S(1)}, bf16[16,48,256]{2,1,0:T(8,128)(2,1)S(1)}, u32[]{:S(2)}, u32[]{:S(2)}) collective-permute-start(bf16[16,48,256]{2,1,0:T(8,128)(2,1)S(1)} %bitcast.54), channel_id=1, source_target_pairs={{0,256},{256,0},{1,257},{257,1},{2,258},{258,2},{3,259},{259,3},{4... | collective-permute-start | bytes 1179656 | tf_op jit(solution)/shard_map/ppermute | solution.py:48
  99.5 19.3 %collective-permute-start.1 = (bf16[8,96,256]{2,1,0:T(8,128)(2,1)S(1)}, bf16[8,96,256]{2,1,0:T(8,128)(2,1)S(1)}, u32[]{:S(2)}, u32[]{:S(2)}) collective-permute-start(bf16[8,96,256]{2,1,0:T(8,128)(2,1)S(1)} %get-tuple-element.11), channel_id=1, source_target_pairs={{0,8},{8,16},{16,24},{24,32},{32,40},{40,48},{48,56},{56,64},{64,7... | collective-permute-start | bytes 1179656 | tf_op jit(solution)/shard_map/ppermute | solution.py:29
  102.8 16.1 %collective-permute-start.2 = (bf16[8,96,256]{2,1,0:T(8,128)(2,1)S(1)}, bf16[8,96,256]{2,1,0:T(8,128)(2,1)S(1)}, u32[]{:S(2)}, u32[]{:S(2)}) collective-permute-start(bf16[8,96,256]{2,1,0:T(8,128)(2,1)S(1)} %get-tuple-element.12), channel_id=1, source_target_pairs={{0,248},{8,0},{16,8},{24,16},{32,24},{40,32},{48,40},{56,48},{64,5... | collective-permute-start | bytes 1179656 | tf_op jit(solution)/shard_map/ppermute | solution.py:29
  119.5 1.1 copy-start
  121.8 1.1 copy-start.5
  134.8 14.1 %copy-start.2 = (bf16[4,512,128]{2,1,0:T(8,128)(2,1)}, bf16[4,512,128]{2,1,0:T(8,128)(2,1)S(1)}, u32[]{:S(2)}) copy-start(bf16[4,512,128]{2,1,0:T(8,128)(2,1)S(1)} %all_to_all.20.mine_ref) | copy-start | bytes 1572868
  134.8 14.1 %collective-permute-start.3 = (bf16[4,512,128]{2,1,0:T(8,128)(2,1)S(1)}, bf16[4,512,128]{2,1,0:T(8,128)(2,1)S(1)}, u32[]{:S(2)}, u32[]{:S(2)}) collective-permute-start(bf16[4,512,128]{2,1,0:T(8,128)(2,1)S(1)} %all_to_all.20.mine_ref), channel_id=1, source_target_pairs={{0,1},{1,0},{2,3},{3,2},{4,5},{5,4},{6,7},{7,6},{8,9},{9,8},{10,11... | collective-permute-start | bytes 1572872 | tf_op jit(solution)/shard_map/ppermute | solution.py:66
  148.9 0.8 copy-start.4
  149.7 25.7 %copy-start.10 = (bf16[2048]{0:T(1024)(128)(2,1)S(1)}, bf16[2048]{0:T(1024)(128)(2,1)}, u32[]{:S(2)}) copy-start(bf16[2048]{0:T(1024)(128)(2,1)} %param.19) | copy-start | bytes 12292
  172.4 5.3 %copy-start.1 = (bf16[4,512,256]{2,1,0:T(8,128)(2,1)}, bf16[4,512,256]{2,1,0:T(8,128)(2,1)S(1)}, u32[]{:S(2)}) copy-start(bf16[4,512,256]{2,1,0:T(8,128)(2,1)S(1)} %all_to_all.21.mine_ref) | copy-start | bytes 3145732
  172.4 5.3 %collective-permute-start.4 = (bf16[4,512,256]{2,1,0:T(8,128)(2,1)S(1)}, bf16[4,512,256]{2,1,0:T(8,128)(2,1)S(1)}, u32[]{:S(2)}, u32[]{:S(2)}) collective-permute-start(bf16[4,512,256]{2,1,0:T(8,128)(2,1)S(1)} %all_to_all.21.mine_ref), channel_id=1, source_target_pairs={{0,1},{1,0},{2,3},{3,2},{4,5},{5,4},{6,7},{7,6},{8,9},{9,8},{10,11... | collective-permute-start | bytes 3145736 | tf_op jit(solution)/shard_map/ppermute | solution.py:66
  177.7 1.0 copy-start.3
  194.1 14.3 %collective-permute-start.5 = (bf16[4,512,256]{2,1,0:T(8,128)(2,1)}, bf16[4,512,256]{2,1,0:T(8,128)(2,1)S(1)}, u32[]{:S(2)}, u32[]{:S(2)}) collective-permute-start(bf16[4,512,256]{2,1,0:T(8,128)(2,1)} %get-tuple-element.8), channel_id=1, source_target_pairs={{0,1},{1,0},{2,3},{3,2},{4,5},{5,4},{6,7},{7,6},{8,9},{9,8},{10,11... | collective-permute-start | bytes 3145736 | tf_op jit(solution)/shard_map/ppermute | solution.py:66
Sparse Core Ops, SparseCore 0:
  9.4 167.7 all-gather.2
